TPU v7x, 32 devices: a whole 2x2x4 slice. The times are simulated.
32 devices in a mesh: grp: 2 (over y), fs: 4 (over z), tp: 4 (over x, core).
Axes of the slice: x: 2, y: 2, z: 4, core: 2. Of those that a mesh axis runs over, the one named last changes fastest.
Arguments:
- tokens: bfloat16 [1024, 2048], P(('grp', 'fs'), 'tp'), parts along dimension 0, may hold values from -340 to 340
- routes: int32 [1024, 2], P(('grp', 'fs')), parts along dimension 0, may hold values from 0 to 7, all different within a row; in each aligned block of 128 rows (0 to 127, 128 to 255, ...) at most 40 rows name the same one
- route_weights: float32 [1024, 2], P(('grp', 'fs')), parts along dimension 0, may hold values from 0.2 to 1
- norm_gain: float32 [2048], P('fs'), may hold values from 0.1 to 1.9
- gate_weight: float32 [8, 2048, 4096], P(None, 'fs', 'tp'), may hold values from -0.125 to 0.125
- up_weight: float32 [8, 2048, 4096], P(None, 'fs', 'tp'), may hold values from -0.125 to 0.125
- down_weight: float32 [8, 2048, 4096], P(None, 'fs', 'tp'), may hold values from -0.09375 to 0.09375
Outputs:
- gate_out: bfloat16 [8, 4096, 4096], P('fs', 'grp', 'tp'), parts along dimension 1
- up_out: bfloat16 [8, 4096, 4096], P('fs', 'grp', 'tp'), parts along dimension 1
- down_out: bfloat16 [8, 4096, 4096], P('fs', 'grp', 'tp'), parts along dimension 1
- mixed_out: bfloat16 [1024, 2048], P(('grp', 'fs'), 'tp'), parts along dimension 0
There are 2 independent parts, one for each index of `grp`. A program takes and returns all parts, laid end to end along the dimension named above; an argument that names none is the same for every part. Nothing has to cross between parts.
Inputs may be any that keep to these rules, and one draw needn't show every extreme that they name: `routes`: each row names 2 different experts; in each aligned block of 128 rows no expert is named by more than 40 rows, and in some block one expert is named by exactly 40 rows.
All inputs are finite; a program needn't handle non-finite values.
Results may differ from a plain program's by a relative error of at most 0.015.
Values may be sent and summed in bfloat16 or wider, within the bound.
A program may use at most 192 MiB of HBM per device.

v0:
```python
import jax
import jax.numpy as jnp
from jax import lax
from jax.sharding import PartitionSpec as P

epsilon = 1e-06


def expert_slots(routes, experts, capacity):
    row_count = routes.shape[0] * routes.shape[1]
    flat_routes = routes.reshape(row_count)
    onehot = (flat_routes[:, None] == jnp.arange(experts, dtype=jnp.int32)[None, :]).astype(
        jnp.int32
    )
    earlier = jnp.cumsum(onehot, axis=0) - onehot
    position = jnp.sum(earlier * onehot, axis=1)
    return (flat_routes * capacity + position).reshape(routes.shape)


def dispatch(normed, slots, experts, capacity, copies, local_count):
    col_width = normed.shape[1]
    slot_ids = jnp.arange(experts * capacity, dtype=jnp.int32)
    select = jnp.any(slot_ids[:, None, None] == slots[None, :, :], axis=2).astype(jnp.bfloat16)
    packed = jnp.dot(select, normed, preferred_element_type=jnp.float32).astype(jnp.bfloat16)
    packed = jnp.broadcast_to(
        packed.reshape(experts, 1, capacity, col_width), (experts, copies, capacity, col_width)
    )
    return packed.reshape(experts * copies // local_count, local_count, capacity, col_width)


def combine(returned, slots, route_weights, experts, copies):
    capacity, col_width = (returned.shape[2], returned.shape[3])
    summed_up = jnp.sum(
        returned.reshape(experts, copies, capacity, col_width), axis=1, dtype=jnp.float32
    )
    selected = summed_up.reshape(experts * capacity, col_width)[slots]
    return jnp.sum(route_weights[:, :, None] * selected, axis=1)


def on_device(tokens, routes, route_weights, norm_gain, gate_weight, up_weight, down_weight):
    fs_count = lax.axis_size("fs")
    tp_count = lax.axis_size("tp")
    experts = gate_weight.shape[0]
    copies = max(1, fs_count // experts)
    local_count = max(1, experts // fs_count)
    capacity = tokens.shape[0] * 5 // 16
    block_width = gate_weight.shape[2] // copies

    def pieces(matrix):
        localized = matrix.reshape(experts, matrix.shape[1], copies, block_width)
        return jnp.transpose(localized, (0, 2, 1, 3)).reshape(
            experts * copies, matrix.shape[1], block_width
        )

    gain_row = norm_gain[None, :, None]
    gate_new, up_new, down_new = (
        lax.all_to_all(
            pieces((gain_row * gate_weight).astype(jnp.bfloat16)),
            "fs",
            split_axis=0,
            concat_axis=1,
            tiled=True,
        ),
        lax.all_to_all(
            pieces((gain_row * up_weight).astype(jnp.bfloat16)),
            "fs",
            split_axis=0,
            concat_axis=1,
            tiled=True,
        ),
        lax.all_to_all(
            pieces(down_weight.astype(jnp.bfloat16)), "fs", split_axis=0, concat_axis=1, tiled=True
        ),
    )
    slots = expert_slots(routes, experts, capacity)
    whole = lax.all_gather(tokens, "tp", axis=1, tiled=True)
    widened = whole.astype(jnp.float32)
    row_scale = lax.rsqrt(jnp.mean(widened * widened, axis=1, keepdims=True) + epsilon)
    normed = (widened * row_scale).astype(jnp.bfloat16)
    outgoing = dispatch(normed, slots, experts, capacity, copies, local_count)
    arrived = lax.all_to_all(outgoing, "fs", split_axis=0, concat_axis=0, tiled=True)
    gate_sums = jnp.einsum("slcd,ldf->slcf", arrived, gate_new, preferred_element_type=jnp.float32)
    up_sums = jnp.einsum("slcd,ldf->slcf", arrived, up_new, preferred_element_type=jnp.float32)
    hidden = (jax.nn.silu(gate_sums) * up_sums).astype(jnp.bfloat16)
    partial_value = jnp.einsum(
        "slcf,ldf->slcd", hidden, down_new, preferred_element_type=jnp.float32
    ).astype(jnp.bfloat16)
    by_columns = partial_value.reshape(
        partial_value.shape[:3] + (tp_count, partial_value.shape[3] // tp_count)
    )
    exchanged = lax.all_to_all(by_columns, "tp", split_axis=3, concat_axis=3, tiled=True)
    summed_up = jnp.sum(exchanged, axis=3, dtype=jnp.float32)
    handed = lax.all_to_all(
        summed_up.astype(jnp.bfloat16), "fs", split_axis=0, concat_axis=0, tiled=True
    ).astype(summed_up.dtype)
    combined = combine(handed, slots, route_weights, experts, copies)
    return (gate_new, up_new, down_new, combined.astype(jnp.bfloat16))


def solution(mesh):
    in_specs = (
        P(("grp", "fs"), "tp"),
        P(("grp", "fs"), None),
        P(("grp", "fs"), None),
        P("fs"),
        P(None, "fs", "tp"),
        P(None, "fs", "tp"),
        P(None, "fs", "tp"),
    )
    out_specs = (
        P("fs", "grp", "tp"),
        P("fs", "grp", "tp"),
        P("fs", "grp", "tp"),
        P(("grp", "fs"), "tp"),
    )
    return jax.shard_map(
        on_device, mesh=mesh, in_specs=in_specs, out_specs=out_specs, check_vma=False
    )
```

profile of v0, /device:TPU:0, one launch (start us, length us, event | category | flops | bytes accessed | tf_op | source)
XLA Modules:
  0.0 669.7 jit_solution(16620702080350999131)
XLA Ops:
  0.6 15.2 %multiply_convert_fusion = (bf16[8,512,1024]{2,1,0:T(8,128)(2,1)}, bf16[8,512,1024]{2,1,0:T(8,128)(2,1)S(1)}) fusion(f32[8,512,1024]{2,1,0:T(8,128)} %param.12, f32[512]{0:T(512)} %param.10, f32[8,512,1024]{2,1,0:T(8,128)} %param.11), kind=kLoop, calls=%fused_computation.1 | loop fusion | flops 16777216 | bytes 50333696 | tf_op jit(solution)/shard_map/convert_element_type | solution.py:65
  15.8 189.3 %all_to_all.69 = bf16[8,512,1024]{2,1,0:T(8,128)(2,1)} all-to-all(bf16[8,512,1024]{2,1,0:T(8,128)(2,1)S(1)} %get-tuple-element.7), channel_id=1, replica_groups=mesh['grp'=2,'fs'=4,'tp'=4] {'fs'}, dimensions={0} | all-to-all | bytes 16777216 | tf_op jit(solution)/shard_map/all_to_all | solution.py:57
  205.1 5.7 all-to-all-start.1
  210.7 9.1 %convert_element_type.43 = bf16[8,512,1024]{2,1,0:T(8,128)(2,1)} convert(f32[8,512,1024]{2,1,0:T(8,128)} %param.13) | non-fusion elementwise | flops 4194304 | bytes 25165824 | tf_op jit(solution)/shard_map/convert_element_type | solution.py:72
  219.8 0.0 copy-start.1
  219.8 0.0 copy-start
  219.8 173.2 %all-to-all-done.1 = bf16[8,512,1024]{2,1,0:T(8,128)(2,1)} async-done(((bf16[8,512,1024]{2,1,0:T(8,128)(2,1)}), bf16[8,512,1024]{2,1,0:T(8,128)(2,1)}, u32[]{:S(2)}, u32[]{:S(2)}) %all-to-all-start.1) | async-done | bytes 8388640 | tf_op jit(solution)/shard_map/all_to_all | solution.py:64
  393.0 5.7 all-to-all-start.2
  398.7 0.0 copy-done.1
  398.7 0.1 copy.70
  398.8 0.1 eq.43
  399.0 0.1 eq.39
  399.1 0.6 reduce-window.6
  399.7 0.2 slice_reduce_fusion
  400.0 0.1 fusion.17
  400.1 0.1 reduce_sum.46
  400.2 0.1 copy.72
  400.3 0.1 fusion.15
  400.3 0.0 copy-done
  400.4 7.2 %all_gather.3 = bf16[128,2048]{1,0:T(8,128)(2,1)S(1)} all-gather(bf16[128,512]{1,0:T(8,128)(2,1)S(1)} %copy-done), channel_id=1, replica_groups=mesh['grp'=2,'fs'=4,'tp'=4] {'tp'}, dimensions={1}, use_global_device_ids=true | all-gather | bytes 655360 | tf_op jit(solution)/shard_map/all_gather | solution.py:76
  407.5 0.2 fusion.10
  407.7 1.8 convolution_convert_fusion
  409.5 171.9 %all-to-all-done.2 = bf16[8,512,1024]{2,1,0:T(8,128)(2,1)} async-done(((bf16[8,512,1024]{2,1,0:T(8,128)(2,1)}), bf16[8,512,1024]{2,1,0:T(8,128)(2,1)}, u32[]{:S(2)}, u32[]{:S(2)}) %all-to-all-start.2) | async-done | bytes 8388640 | tf_op jit(solution)/shard_map/all_to_all | solution.py:71
  581.3 3.7 all-to-all-start.3
  585.1 7.8 %copy.66 = bf16[4,2,512,1024]{3,2,0,1:T(8,128)(2,1)} copy(bf16[4,2,512,1024]{3,2,1,0:T(8,128)(2,1)} %bitcast.55) | data formatting | bytes 16777216 | tf_op jit(solution)/shard_map/all_to_all | solution.py:57
  592.8 7.8 %copy.67 = bf16[4,2,512,1024]{3,2,0,1:T(8,128)(2,1)} copy(bf16[4,2,512,1024]{3,2,1,0:T(8,128)(2,1)} %bitcast.3) | data formatting | bytes 16777216 | tf_op jit(solution)/shard_map/all_to_all | solution.py:64
  600.6 7.8 %copy.68 = bf16[4,2,512,1024]{3,2,0,1:T(8,128)(2,1)} copy(bf16[4,2,512,1024]{3,2,1,0:T(8,128)(2,1)} %bitcast.6) | data formatting | bytes 16777216 | tf_op jit(solution)/shard_map/all_to_all | solution.py:71
  608.3 7.4 %all-to-all-done.3 = bf16[4,2,40,2048]{3,2,1,0:T(8,128)(2,1)S(1)} async-done(((bf16[4,2,40,2048]{3,2,1,0:T(8,128)(2,1)}), bf16[4,2,40,2048]{3,2,1,0:T(8,128)(2,1)S(1)}, u32[]{:S(2)}, u32[]{:S(2)}) %all-to-all-start.3) | async-done | bytes 1310752 | tf_op jit(solution)/shard_map/all_to_all | solution.py:81
  615.8 6.0 convolution_bitcast_fusion.1
  621.7 10.6 %convolution_convert_fusion.1 = bf16[2,4,40,2048]{3,2,1,0:T(8,128)(2,1)S(1)} fusion(bf16[2,2048,1024,1]{2,1,3,0:T(8,128)(2,1)} %bitcast.60, bf16[2,2048,1024,1]{2,1,3,0:T(8,128)(2,1)} %bitcast.58, f32[4,2,40,1024]{3,2,0,1:T(8,128)} %convolution_bitcast_fusion.1, bf16[4,2,40,2048]{3,2,1,0:T(8,128)(2,1)S(1)} %all-to-all-done.3), kind=kOutput, calls=%fused_computation.4 | convolution fusion | flops 2686976000 | bytes 20709376 | tf_op jit(solution)/shard_map/slcf,ldf->slcd/dot_general | solution.py:85
  632.4 0.1 copy.90
  632.5 0.0 copy-start.2
  632.5 19.8 %all_to_all.70 = bf16[4,2,40,4,512]{4,2,0,1,3:T(8,128)(2,1)S(1)} all-to-all(bf16[4,2,40,4,512]{4,2,0,1,3:T(8,128)(2,1)S(1)} %bitcast.62), channel_id=1, replica_groups=mesh['grp'=2,'fs'=4,'tp'=4] {'tp'}, dimensions={3} | all-to-all | bytes 2621440 | tf_op jit(solution)/shard_map/all_to_all | solution.py:91
  652.3 0.3 reduce_sum.48
  652.6 0.7 copy.77
  653.3 3.5 all-to-all-start.5
  656.8 0.1 copy.78
  656.9 0.1 reshape.65
  657.1 0.0 copy-done.2
  657.1 0.1 copy.69
  657.2 9.8 %all-to-all-done.5 = bf16[4,2,40,512]{3,2,1,0:T(8,128)(2,1)S(1)} async-done(((bf16[4,2,40,512]{3,2,1,0:T(8,128)(2,1)}), bf16[4,2,40,512]{3,2,1,0:T(8,128)(2,1)S(1)}, u32[]{:S(2)}, u32[]{:S(2)}) %all-to-all-start.5) | async-done | bytes 327712 | tf_op jit(solution)/shard_map/all_to_all | solution.py:93
  667.0 0.1 bitcast_convert_fusion
  667.1 1.0 gather_fusion
  668.1 0.3 reshape.64
  668.4 1.4 multiply_reduce_fusion
  (6 shorter events, 0.1 us)
Async XLA Ops:
  205.1 187.9 %all-to-all-start.1 = ((bf16[8,512,1024]{2,1,0:T(8,128)(2,1)}), bf16[8,512,1024]{2,1,0:T(8,128)(2,1)}, u32[]{:S(2)}, u32[]{:S(2)}) async-start(bf16[8,512,1024]{2,1,0:T(8,128)(2,1)} %get-tuple-element.6), calls=%async_computation.1 | async-start | bytes 16777216 | tf_op jit(solution)/shard_map/all_to_all | solution.py:64
  219.8 178.9 %copy-start.1 = (s32[128,2]{0,1:T(2,128)S(1)}, s32[128,2]{0,1:T(2,128)}, u32[]{:S(2)}) copy-start(s32[128,2]{0,1:T(2,128)} %param.8) | copy-start | bytes 3076
  219.8 180.6 %copy-start = (bf16[128,512]{1,0:T(8,128)(2,1)S(1)}, bf16[128,512]{1,0:T(8,128)(2,1)}, u32[]{:S(2)}) copy-start(bf16[128,512]{1,0:T(8,128)(2,1)} %param.7) | copy-start | bytes 393220
  393.0 188.3 %all-to-all-start.2 = ((bf16[8,512,1024]{2,1,0:T(8,128)(2,1)}), bf16[8,512,1024]{2,1,0:T(8,128)(2,1)}, u32[]{:S(2)}, u32[]{:S(2)}) async-start(bf16[8,512,1024]{2,1,0:T(8,128)(2,1)} %convert_element_type.43), calls=%async_computation.2 | async-start | bytes 16777216 | tf_op jit(solution)/shard_map/all_to_all | solution.py:71
  581.3 34.4 %all-to-all-start.3 = ((bf16[4,2,40,2048]{3,2,1,0:T(8,128)(2,1)}), bf16[4,2,40,2048]{3,2,1,0:T(8,128)(2,1)S(1)}, u32[]{:S(2)}, u32[]{:S(2)}) async-start(bf16[4,2,40,2048]{3,2,1,0:T(8,128)(2,1)} %bitcast.14), calls=%async_computation.3 | async-start | bytes 2621440 | tf_op jit(solution)/shard_map/all_to_all | solution.py:81
  632.5 24.6 %copy-start.2 = (f32[128,2]{0,1:T(2,128)S(1)}, f32[128,2]{0,1:T(2,128)}, u32[]{:S(2)}) copy-start(f32[128,2]{0,1:T(2,128)} %param.9) | copy-start | bytes 3076
  653.3 13.7 %all-to-all-start.5 = ((bf16[4,2,40,512]{3,2,1,0:T(8,128)(2,1)}), bf16[4,2,40,512]{3,2,1,0:T(8,128)(2,1)S(1)}, u32[]{:S(2)}, u32[]{:S(2)}) async-start(bf16[4,2,40,512]{3,2,1,0:T(8,128)(2,1)} %copy.77), calls=%async_computation.5 | async-start | bytes 655360 | tf_op jit(solution)/shard_map/all_to_all | solution.py:93
where the time goes:
time: 670 us
  waiting for transfers between devices  362 us (54%)
  blocking collectives  216 us (32%)
  other arithmetic  27 us (4%)
  local copies, waits for them, and re-layouts  26.6 us (4%)
  starting transfers between devices  18.5 us (3%)
  matrix products  18.4 us (3%)
    all_to_all x1, blocking collectives, on_device(): lax.all_to_all(pieces((gain_row * gate_weight).astype(jnp.bfloat16)), 'fs...  189 us
    all_to_all x1, waiting for transfers between devices, on_device(): lax.all_to_all(pieces((gain_row * up_weight).astype(jnp.bfloat16)), 'fs',...  173 us
    all_to_all x1, waiting for transfers between devices, on_device(): lax.all_to_all(pieces(down_weight.astype(jnp.bfloat16)), 'fs', split_axis...  172 us
    all_to_all x1, blocking collectives, on_device(): lax.all_to_all(by_columns, 'tp', split_axis=3, concat_axis=3, tiled=True)  19.8 us
    convert_element_type x1, other arithmetic, on_device(): (gain_row * up_weight).astype(jnp.bfloat16)  15.2 us
  transfers between devices with their start and end apart: 4, of which 4 were waited for; matrix products, arithmetic and copies ran while one was open for 5% of the time, Pallas kernels for 0%

commit v1 on v0

--- a/solution.py
+++ b/solution.py
@@ -1,9 +1,14 @@
+import functools
+
 import jax
 import jax.numpy as jnp
 from jax import lax
+from jax.experimental import pallas as pl
+from jax.experimental.pallas import tpu as pltpu
 from jax.sharding import PartitionSpec as P
 
 epsilon = 1e-06
+MESH = pl.DeviceIdType.MESH
 
 
 def expert_slots(routes, experts, capacity):
@@ -37,40 +42,218 @@
     return jnp.sum(route_weights[:, :, None] * selected, axis=1)
 
 
+def exchange_kernel(
+    dims, gains, gate_w, up_w, down_w, gate_o, up_o, down_o,
+    raw, stage, load_sem, send_sem, recv_sem, pass_send, pass_recv,
+):
+    groups, count, local, copies, rows, width, parts = dims
+    weights, landing = (gate_w, up_w, down_w), (gate_o, up_o, down_o)
+    y, z = lax.axis_index("grp"), lax.axis_index("fs")
+    share = rows // groups
+    piece = share // parts
+
+    barrier = pltpu.get_barrier_semaphore()
+
+    def greet(j, _):
+        @pl.when(j != z)
+        def _():
+            pl.semaphore_signal(barrier, inc=1, device_id={"fs": j}, device_id_type=MESH)
+        return 0
+
+    lax.fori_loop(0, count, greet, 0)
+    for other in range(1, groups):
+        pl.semaphore_signal(
+            barrier, inc=1, device_id={"grp": lax.rem(y + other, groups)}, device_id_type=MESH
+        )
+
+    def load(m, j, first, slot):
+        if copies > 1:
+            expert, column = j // copies, lax.rem(j, copies) * width
+            column = pl.ds(pl.multiple_of(column, 128), width)
+        else:
+            expert, column = j * local, slice(None)
+        return pltpu.make_async_copy(
+            weights[m].at[pl.ds(expert, local), pl.ds(first, share), column],
+            raw.at[slot], load_sem.at[slot],
+        )
+
+    def fold(m, slot, first, put):
+        def one(i, _):
+            l, q = i // parts, lax.rem(i, parts)
+            at = pl.multiple_of(q * piece, piece)
+            scaled = raw[slot, l, pl.ds(at, piece), :]
+            if m < 2:
+                scaled = scaled * gains[pl.ds(pl.multiple_of(first + at, piece), piece), :1]
+            put(l, at, scaled.astype(jnp.bfloat16))
+            return 0
+
+        lax.fori_loop(0, local * parts, one, 0)
+
+    def sending(j, m, i):
+        l, q = i // parts, lax.rem(i, parts)
+        at = pl.multiple_of(q * piece, piece)
+        base = pl.multiple_of(z * rows + y * share + at, piece)
+        return pltpu.make_async_remote_copy(
+            src_ref=stage.at[j, m, l, pl.ds(at, piece), :],
+            dst_ref=landing[m].at[l, pl.ds(base, piece), :],
+            send_sem=send_sem.at[j, m, i],
+            recv_sem=recv_sem.at[z, m, i],
+            device_id={"fs": j}, device_id_type=MESH,
+        )
+
+    def passing(s, m, i, other):
+        l, q = i // parts, lax.rem(i, parts)
+        base = pl.multiple_of(s * rows + y * share + q * piece, piece)
+        spot = landing[m].at[l, pl.ds(base, piece), :]
+        return pltpu.make_async_remote_copy(
+            src_ref=spot, dst_ref=spot,
+            send_sem=pass_send.at[s, m, i, other - 1],
+            recv_sem=pass_recv.at[s, m, i, other - 1],
+            device_id={"grp": lax.rem(y + other, groups)}, device_id_type=MESH,
+        )
+
+    def arriving(s, m, i, other):
+        l, q = i // parts, lax.rem(i, parts)
+        giver = lax.rem(y + groups - other, groups)
+        base = pl.multiple_of(s * rows + giver * share + q * piece, piece)
+        spot = landing[m].at[l, pl.ds(base, piece), :]
+        return pltpu.make_async_remote_copy(
+            src_ref=spot, dst_ref=spot,
+            send_sem=pass_send.at[s, m, i, other - 1],
+            recv_sem=pass_recv.at[s, m, i, other - 1],
+            device_id={"grp": giver}, device_id_type=MESH,
+        )
+
+    def landed(s, m, i):
+        l, q = i // parts, lax.rem(i, parts)
+        base = pl.multiple_of(s * rows + y * share + q * piece, piece)
+        return pltpu.make_async_remote_copy(
+            src_ref=landing[m].at[l, pl.ds(base, piece), :],
+            dst_ref=landing[m].at[l, pl.ds(base, piece), :],
+            send_sem=send_sem.at[s, m, i],
+            recv_sem=recv_sem.at[s, m, i],
+            device_id={"fs": s}, device_id_type=MESH,
+        )
+
+    mine = pl.multiple_of(y * share, share)
+    pieces = local * parts
+
+    def neighbours(body):
+        def step(d, _):
+            for j, there in ((z + d, z + d < count), (z - d, z - d >= 0)):
+                @pl.when(there)
+                def _():
+                    body(j)
+            return 0
+
+        lax.fori_loop(1, count, step, 0)
+
+    def send_phase(phase):
+        def to(j):
+            for m in phase:
+                load(m, j, mine, m % 2).start()
+            for m in phase:
+                load(m, j, mine, m % 2).wait()
+
+                def put(l, at, value):
+                    stage[j, m, l, pl.ds(at, piece), :] = value
+
+                fold(m, m % 2, mine, put)
+            for m in phase:
+                def go(i, _):
+                    sending(j, m, i).start()
+                    return 0
+
+                lax.fori_loop(0, pieces, go, 0)
+
+        neighbours(to)
+
+    pl.semaphore_wait(barrier, count - 1 + groups - 1)
+    send_phase((0, 1))
+    send_phase((2,))
+
+    for m in range(3):
+        for g in range(groups):
+            load(m, z, g * share, g % 2).start()
+            load(m, z, g * share, g % 2).wait()
+
+            def put(l, at, value):
+                base = pl.multiple_of(z * rows + g * share + at, piece)
+                landing[m][l, pl.ds(base, piece), :] = value
+
+            fold(m, g % 2, g * share, put)
+
+    def pass_phase(phase):
+        def take(s):
+            for m in phase:
+                def one(i, _):
+                    landed(s, m, i).wait_recv()
+                    for other in range(1, groups):
+                        passing(s, m, i, other).start()
+                    return 0
+
+                lax.fori_loop(0, pieces, one, 0)
+
+        neighbours(take)
+
+    pass_phase((0, 1))
+    pass_phase((2,))
+
+    def finish(s):
+        for m in range(3):
+            def one(i, _):
+                for other in range(1, groups):
+                    arriving(s, m, i, other).wait_recv()
+                    passing(s, m, i, other).wait_send()
+                sending(s, m, i).wait_send()
+                return 0
+
+            lax.fori_loop(0, pieces, one, 0)
+
+    neighbours(finish)
+
+
+def exchange(norm_gain, gate_weight, up_weight, down_weight, groups, count, copies, local):
+    experts, rows, columns = gate_weight.shape
+    width = columns // copies
+    share = rows // groups
+    parts = max(1, share // 128)
+    gains = jnp.broadcast_to(norm_gain[:, None], (rows, 128))
+    shape = (local, count * rows, width)
+    dims = (groups, count, local, copies, rows, width, parts)
+    pieces = local * parts
+    return pl.pallas_call(
+        functools.partial(exchange_kernel, dims),
+        out_shape=[jax.ShapeDtypeStruct(shape, jnp.bfloat16)] * 3,
+        in_specs=[pl.BlockSpec(memory_space=pltpu.VMEM)]
+        + [pl.BlockSpec(memory_space=pl.ANY)] * 3,
+        out_specs=[pl.BlockSpec(memory_space=pltpu.VMEM)] * 3,
+        scratch_shapes=[
+            pltpu.VMEM((2, local, share, width), jnp.float32),
+            pltpu.VMEM((count, 3, local, share, width), jnp.bfloat16),
+            pltpu.SemaphoreType.DMA((2,)),
+            pltpu.SemaphoreType.DMA((count, 3, pieces)),
+            pltpu.SemaphoreType.DMA((count, 3, pieces)),
+            pltpu.SemaphoreType.DMA((count, 3, pieces, max(1, groups - 1))),
+            pltpu.SemaphoreType.DMA((count, 3, pieces, max(1, groups - 1))),
+        ],
+        compiler_params=pltpu.CompilerParams(
+            collective_id=0, has_side_effects=True, vmem_limit_bytes=60 * 1024 * 1024
+        ),
+    )(gains, gate_weight, up_weight, down_weight)
+
+
 def on_device(tokens, routes, route_weights, norm_gain, gate_weight, up_weight, down_weight):
+    groups = lax.axis_size("grp")
     fs_count = lax.axis_size("fs")
     tp_count = lax.axis_size("tp")
     experts = gate_weight.shape[0]
     copies = max(1, fs_count // experts)
     local_count = max(1, experts // fs_count)
     capacity = tokens.shape[0] * 5 // 16
-    block_width = gate_weight.shape[2] // copies
-
-    def pieces(matrix):
-        localized = matrix.reshape(experts, matrix.shape[1], copies, block_width)
-        return jnp.transpose(localized, (0, 2, 1, 3)).reshape(
-            experts * copies, matrix.shape[1], block_width
-        )
-
-    gain_row = norm_gain[None, :, None]
-    gate_new, up_new, down_new = (
-        lax.all_to_all(
-            pieces((gain_row * gate_weight).astype(jnp.bfloat16)),
-            "fs",
-            split_axis=0,
-            concat_axis=1,
-            tiled=True,
-        ),
-        lax.all_to_all(
-            pieces((gain_row * up_weight).astype(jnp.bfloat16)),
-            "fs",
-            split_axis=0,
-            concat_axis=1,
-            tiled=True,
-        ),
-        lax.all_to_all(
-            pieces(down_weight.astype(jnp.bfloat16)), "fs", split_axis=0, concat_axis=1, tiled=True
-        ),
+
+    gate_new, up_new, down_new = exchange(
+        norm_gain, gate_weight, up_weight, down_weight, groups, fs_count, copies, local_count
     )
     slots = expert_slots(routes, experts, capacity)
     whole = lax.all_gather(tokens, "tp", axis=1, tiled=True)

time: 670 us -> 480 us (0.72)
  Pallas kernels: 0 us -> 385 us
  waiting for transfers between devices: 362 us -> 9.63 us
  blocking collectives: 216 us -> 28.5 us
  other arithmetic: 27 us -> 3.42 us
  starting transfers between devices: 18.5 us -> 8.64 us
    pallas_call x0 -> x1, Pallas kernels: none -> 385 us  [exchange(): pl.pallas_call(functools.partial(exchange_kernel, dims), out_shape=[jax.S...]
    all_to_all x2 -> x0, waiting for transfers between devices: 345 us -> none  [the longest x1 173 us: on_device(): lax.all_to_all(pieces((gain_row * up_weight).astype(jnp.bfloat16)), 'fs',...]
    all_to_all x1 -> x0, blocking collectives: 189 us -> none  [on_device(): lax.all_to_all(pieces((gain_row * gate_weight).astype(jnp.bfloat16)), 'fs...]
    convert_element_type x2 -> x0, other arithmetic: 24.2 us -> none  [the longest x1 15.2 us: on_device(): (gain_row * up_weight).astype(jnp.bfloat16)]
    unnamed x8 -> x13, local copies, waits for them, and re-layouts: 0.24 us -> 24.2 us
    all_to_all x3 -> x0, local copies, waits for them, and re-layouts: 23.3 us -> none  [the longest x1 7.76 us: on_device(): lax.all_to_all(pieces((gain_row * gate_weight).astype(jnp.bfloat16)), 'fs...]
    all_to_all x2 -> x0, starting transfers between devices: 11.4 us -> none  [the longest x1 5.7 us: on_device(): lax.all_to_all(pieces(down_weight.astype(jnp.bfloat16)), 'fs', split_axis...]
    dot_general x1, matrix products: 10.6 us -> 2.91 us  [on_device(): jnp.einsum('slcf,ldf->slcd', hidden, down_new, preferred_element_type=jnp...]
  transfers between devices with their start and end apart: 4 -> 2, of which waited for: 4 -> 1; matrix products, arithmetic and copies ran while one was open for 5% -> 0% of each run, Pallas kernels for 0% -> 80%
where the time goes in v1:
time: 480 us; the launch traced here: 479 us
  Pallas kernels  385 us (80%)
  blocking collectives  28.5 us (6%)
  local copies, waits for them, and re-layouts  28.1 us (6%)
  matrix products  14.9 us (3%)
  waiting for transfers between devices  9.63 us (2%)
  starting transfers between devices  8.64 us (2%)
    pallas_call x1, Pallas kernels, exchange(): pl.pallas_call(functools.partial(exchange_kernel, dims), out_shape=[jax.S...  385 us
    unnamed x13, local copies, waits for them, and re-layouts  24.2 us
    all_to_all x1, blocking collectives, on_device(): lax.all_to_all(by_columns, 'tp', split_axis=3, concat_axis=3, tiled=True)  19.7 us
    all_to_all x1, waiting for transfers between devices, on_device(): lax.all_to_all(summed_up.astype(jnp.bfloat16), 'fs', split_axis=0, concat...  9.63 us
  transfers between devices with their start and end apart: 2, of which 1 were waited for; matrix products, arithmetic and copies ran while one was open for 0% of the time, Pallas kernels for 80%

profile of v1, /device:TPU:0, one launch (start us, length us, event | category | flops | bytes accessed | tf_op | source)
XLA Modules:
  0.0 479.3 jit_solution(8996079363100659652)
XLA Ops:
  0.6 0.8 copy.52
  1.4 0.1 eq.43
  1.6 0.1 eq.39
  1.7 0.6 reduce-window.6
  2.3 0.2 slice_reduce_fusion
  2.6 0.1 fusion.29
  2.6 0.1 reduce_sum.46
  2.8 0.1 copy.54
  2.9 0.7 compare_select_fusion
  3.6 8.9 %all_gather.3 = bf16[128,2048]{1,0:T(8,128)(2,1)S(1)} all-gather(bf16[128,512]{1,0:T(8,128)(2,1)} %param.7), channel_id=1, replica_groups=mesh['grp'=2,'fs'=4,'tp'=4] {'tp'}, dimensions={1}, use_global_device_ids=true | all-gather | bytes 655360 | tf_op jit(solution)/shard_map/all_gather | solution.py:259
  12.5 0.2 fusion.23
  12.7 1.6 convolution_convert_fusion
  14.3 0.0 copy-start
  14.3 5.0 %all-to-all-start = ((bf16[4,2,40,2048]{3,2,1,0:T(8,128)(2,1)}), bf16[4,2,40,2048]{3,2,1,0:T(8,128)(2,1)S(1)}, u32[]{:S(2)}, u32[]{:S(2)}) async-start(bf16[4,2,40,2048]{3,2,1,0:T(8,128)(2,1)} %bitcast.6), calls=%async_computation | async-start | bytes 2621440 | tf_op jit(solution)/shard_map/all_to_all | solution.py:264
  19.3 0.0 copy-done
  19.3 0.8 broadcast_in_dim.4.gains
  20.2 385.3 %shard_map.102 = (bf16[2,2048,1024]{2,1,0:T(8,128)(2,1)}, bf16[2,2048,1024]{2,1,0:T(8,128)(2,1)}, bf16[2,2048,1024]{2,1,0:T(8,128)(2,1)}) custom-call(f32[512,128]{1,0:T(8,128)} %broadcast_in_dim.4.gains, f32[8,512,1024]{2,1,0:T(8,128)} %gate_w.1, f32[8,512,1024]{2,1,0:T(8,128)} %up_w.1, f32[8,512,1024]{2,1,0:T(8,128)} %down_w.1), custom_call_target="tpu_custom_call" | custom-call | tf_op jit(solution)/shard_map/pallas_call | solution.py:225
  405.5 0.0 all-to-all-done
  405.5 0.0 slice-start
  405.5 5.0 %fusion.9 = f32[4,2,40,1024]{3,2,0,1:T(8,128)S(1)} fusion(bf16[2,2048,1024]{2,1,0:T(8,128)(2,1)} %get-tuple-element.16, bf16[4,2,40,2048]{3,2,1,0:T(8,128)(2,1)S(1)} %all-to-all-done), kind=kOutput, calls=%fused_computation.9 | convolution fusion | flops 1342177280 | bytes 11010048 | tf_op jit(solution)/shard_map/slcd,ldf->slcf/dot_general | solution.py:265
  410.5 0.0 slice-start.1
  410.5 5.3 %fusion.18 = bf16[4,2,40,1024]{3,2,0,1:T(8,128)(2,1)S(1)} fusion(bf16[2,2048,1024]{2,1,0:T(8,128)(2,1)} %get-tuple-element.17, f32[4,2,40,1024]{3,2,0,1:T(8,128)S(1)} %fusion.9, bf16[4,2,40,2048]{3,2,1,0:T(8,128)(2,1)S(1)} %all-to-all-done), kind=kOutput, calls=%fused_computation.12 | convolution fusion | flops 1344143360 | bytes 11665408 | tf_op jit(solution)/shard_map/slcd,ldf->slcf/dot_general | solution.py:266
  415.8 0.0 slice-done
  415.8 0.0 slice-done.1
  415.9 2.9 fusion.6
  418.8 0.1 copy.71
  418.9 19.7 %all_to_all.15 = bf16[4,2,40,4,512]{4,2,0,1,3:T(8,128)(2,1)S(1)} all-to-all(bf16[4,2,40,4,512]{4,2,0,1,3:T(8,128)(2,1)S(1)} %bitcast.54), channel_id=1, replica_groups=mesh['grp'=2,'fs'=4,'tp'=4] {'tp'}, dimensions={3} | all-to-all | bytes 2621440 | tf_op jit(solution)/shard_map/all_to_all | solution.py:274
  438.6 0.0 copy-start.1
  438.6 0.3 reduce_sum.48
  438.9 0.8 copy.59
  439.6 3.6 all-to-all-start.2
  443.3 0.1 copy.60
  443.4 0.1 reshape.65
  443.5 0.0 copy-done.1
  443.5 0.1 copy.51
  443.7 9.6 %all-to-all-done.2 = bf16[4,2,40,512]{3,2,1,0:T(8,128)(2,1)S(1)} async-done(((bf16[4,2,40,512]{3,2,1,0:T(8,128)(2,1)}), bf16[4,2,40,512]{3,2,1,0:T(8,128)(2,1)S(1)}, u32[]{:S(2)}, u32[]{:S(2)}) %all-to-all-start.2) | async-done | bytes 327712 | tf_op jit(solution)/shard_map/all_to_all | solution.py:276
  453.3 0.1 bitcast_convert_fusion
  453.4 1.0 gather_fusion
  454.4 0.3 reshape.64
  454.7 1.4 multiply_reduce_fusion
  456.1 7.8 %copy.75 = bf16[2,2048,1024]{2,1,0:T(8,128)(2,1)} copy(bf16[2,2048,1024]{2,1,0:T(8,128)(2,1)} %get-tuple-element.16) | data formatting | bytes 16777216
  463.8 7.8 %copy.76 = bf16[2,2048,1024]{2,1,0:T(8,128)(2,1)} copy(bf16[2,2048,1024]{2,1,0:T(8,128)(2,1)} %get-tuple-element.17) | data formatting | bytes 16777216
  471.6 7.8 %copy.77 = bf16[2,2048,1024]{2,1,0:T(8,128)(2,1)} copy(bf16[2,2048,1024]{2,1,0:T(8,128)(2,1)} %get-tuple-element.18) | data formatting | bytes 16777216
  (7 shorter events, 0.1 us)
Async XLA Ops:
  14.3 5.0 %copy-start = (f32[512]{0:T(512)S(1)}, f32[512]{0:T(512)}, u32[]{:S(2)}) copy-start(f32[512]{0:T(512)} %param.10) | copy-start | bytes 6148
  14.3 391.1 %all-to-all-start = ((bf16[4,2,40,2048]{3,2,1,0:T(8,128)(2,1)}), bf16[4,2,40,2048]{3,2,1,0:T(8,128)(2,1)S(1)}, u32[]{:S(2)}, u32[]{:S(2)}) async-start(bf16[4,2,40,2048]{3,2,1,0:T(8,128)(2,1)} %bitcast.6), calls=%async_computation | async-start | bytes 2621440 | tf_op jit(solution)/shard_map/all_to_all | solution.py:264
  405.5 10.4 %slice-start = ((s8[8388608]{0:T(1024)(128)(4,1)}), s8[4194304]{0:T(1024)(128)(4,1)S(1)}, s32[]{:S(2)}) async-start(s8[8388608]{0:T(1024)(128)(4,1)} %bitcast.52), calls=%async_computation.3 | async-start | bytes 8388608
  410.5 5.3 %slice-start.1 = ((s8[8388608]{0:T(1024)(128)(4,1)}), s8[4194304]{0:T(1024)(128)(4,1)S(1)}, s32[]{:S(2)}) async-start(s8[8388608]{0:T(1024)(128)(4,1)} %bitcast.52), calls=%async_computation.4 | async-start | bytes 8388608
  438.6 5.0 %copy-start.1 = (f32[128,2]{0,1:T(2,128)S(1)}, f32[128,2]{0,1:T(2,128)}, u32[]{:S(2)}) copy-start(f32[128,2]{0,1:T(2,128)} %param.9) | copy-start | bytes 3076
  439.6 13.7 %all-to-all-start.2 = ((bf16[4,2,40,512]{3,2,1,0:T(8,128)(2,1)}), bf16[4,2,40,512]{3,2,1,0:T(8,128)(2,1)S(1)}, u32[]{:S(2)}, u32[]{:S(2)}) async-start(bf16[4,2,40,512]{3,2,1,0:T(8,128)(2,1)} %copy.59), calls=%async_computation.2 | async-start | bytes 655360 | tf_op jit(solution)/shard_map/all_to_all | solution.py:276

commit v2 on v1

--- a/solution.py
+++ b/solution.py
@@ -213,6 +213,241 @@
     neighbours(finish)
 
 
+def relay_kernel(
+    dims, gains, gate_w, up_w, down_w, gate_o, up_o, down_o,
+    raw, stage, transit, load_sem, send_sem, recv_sem, relay_sem, pass_send, pass_recv,
+):
+    groups, count, local, copies, rows, width, parts = dims
+    weights, landing = (gate_w, up_w, down_w), (gate_o, up_o, down_o)
+    y, z = lax.axis_index("grp"), lax.axis_index("fs")
+    share = rows // groups
+    piece = share // parts
+    pieces = local * parts
+    mine = pl.multiple_of(y * share, share)
+
+    def real(way, place):
+        return place if way == 0 else count - 1 - place
+
+    barrier = pltpu.get_barrier_semaphore()
+    for j, there in ((z + 1, z + 1 < count), (z - 1, z >= 1)):
+        @pl.when(there)
+        def _():
+            pl.semaphore_signal(barrier, inc=1, device_id={"fs": j}, device_id_type=MESH)
+    for other in range(1, groups):
+        pl.semaphore_signal(
+            barrier, inc=1, device_id={"grp": lax.rem(y + other, groups)}, device_id_type=MESH
+        )
+
+    def load(m, j, first, slot):
+        if copies > 1:
+            expert, column = j // copies, lax.rem(j, copies) * width
+            column = pl.ds(pl.multiple_of(column, 128), width)
+        else:
+            expert, column = j * local, slice(None)
+        return pltpu.make_async_copy(
+            weights[m].at[pl.ds(expert, local), pl.ds(first, share), column],
+            raw.at[slot], load_sem.at[slot],
+        )
+
+    def cut(i):
+        return i // parts, pl.multiple_of(lax.rem(i, parts) * piece, piece)
+
+    def fold(m, slot, first, put):
+        def one(i, _):
+            l, at = cut(i)
+            scaled = raw[slot, l, pl.ds(at, piece), :]
+            if m < 2:
+                scaled = scaled * gains[pl.ds(pl.multiple_of(first + at, piece), piece), :1]
+            put(l, at, scaled.astype(jnp.bfloat16))
+            return 0
+
+        lax.fori_loop(0, pieces, one, 0)
+
+    def spot(m, l, at, source, giver):
+        base = pl.multiple_of(source * rows + giver * share + at, piece)
+        return landing[m].at[l, pl.ds(base, piece), :]
+
+    def hop(way, src, sem, m, i, k, s, dd, final):
+        l, at = cut(i)
+        if final:
+            dst = spot(m, l, at, real(way, s), y)
+        else:
+            slot = (k - s) * (count - 2 - k) + (count - 1 - dd)
+            dst = transit.at[way, slot, m, l, pl.ds(at, piece), :]
+        place = (k - s) * (count - 1 - k) + (count - 1 - dd)
+        return pltpu.make_async_remote_copy(
+            src_ref=src, dst_ref=dst, send_sem=sem,
+            recv_sem=recv_sem.at[way, place, m, i],
+            device_id={"fs": real(way, k + 1)}, device_id_type=MESH,
+        )
+
+    def start_hop(way, src, sem, m, i, k, s, dd):
+        @pl.when(dd == k + 1)
+        def _():
+            hop(way, src, sem, m, i, k, s, dd, True).start()
+
+        @pl.when(dd > k + 1)
+        def _():
+            hop(way, src, sem, m, i, k, s, dd, False).start()
+
+    def passing(s, m, i, other):
+        l, at = cut(i)
+        ref = spot(m, l, at, s, y)
+        return pltpu.make_async_remote_copy(
+            src_ref=ref, dst_ref=ref,
+            send_sem=pass_send.at[s, m, i, other - 1],
+            recv_sem=pass_recv.at[s, m, i, other - 1],
+            device_id={"grp": lax.rem(y + other, groups)}, device_id_type=MESH,
+        )
+
+    def arriving(s, m, i, other):
+        l, at = cut(i)
+        giver = lax.rem(y + groups - other, groups)
+        ref = spot(m, l, at, s, giver)
+        return pltpu.make_async_remote_copy(
+            src_ref=ref, dst_ref=ref,
+            send_sem=pass_send.at[s, m, i, other - 1],
+            recv_sem=pass_recv.at[s, m, i, other - 1],
+            device_id={"grp": giver}, device_id_type=MESH,
+        )
+
+    def send_phase(phase):
+        def step(d, _):
+            for way in (0, 1):
+                k = real(way, z)
+                dd = count - d
+                j = real(way, dd)
+
+                @pl.when(dd > k)
+                def _():
+                    for m in phase:
+                        load(m, j, mine, m).start()
+                    for m in phase:
+                        load(m, j, mine, m).wait()
+
+                        def put(l, at, value):
+                            stage[j, m, l, pl.ds(at, piece), :] = value
+
+                        fold(m, m, mine, put)
+
+                        def go(i, _):
+                            l, at = cut(i)
+                            src = stage.at[j, m, l, pl.ds(at, piece), :]
+                            start_hop(way, src, send_sem.at[j, m, i], m, i, k, k, dd)
+                            return 0
+
+                        lax.fori_loop(0, pieces, go, 0)
+            return 0
+
+        lax.fori_loop(1, count, step, 0)
+
+    def own_block():
+        for m in range(3):
+            for g in range(groups):
+                load(m, z, g * share, g % 2).start()
+                load(m, z, g * share, g % 2).wait()
+
+                def put(l, at, value):
+                    stage[z, m, l, pl.ds(at, piece), :] = value
+
+                fold(m, g % 2, g * share, put)
+                base = pl.multiple_of(z * rows + g * share, share)
+                keep = pltpu.make_async_copy(
+                    stage.at[z, m], landing[m].at[:, pl.ds(base, share), :], load_sem.at[g % 2]
+                )
+                keep.start()
+                keep.wait()
+
+    def take_phase(phase):
+        most = max(k * (count - k) for k in range(count))
+
+        def take(item, _):
+            for m in phase:
+                def one(i, _):
+                    l, at = cut(i)
+                    for way in (0, 1):
+                        take_piece(way, m, item, i, l, at)
+                    return 0
+
+                lax.fori_loop(0, pieces, one, 0)
+            return 0
+
+        lax.fori_loop(0, most, take, 0)
+
+    def take_piece(way, m, item, i, l, at):
+        k = real(way, z)
+
+        @pl.when(item < k * (count - k))
+        def _():
+            s = k - 1 - item // (count - k)
+            dd = count - 1 - lax.rem(item, count - k)
+            source = real(way, s)
+
+            def awaited(ref):
+                pltpu.make_async_remote_copy(
+                    src_ref=ref, dst_ref=ref, send_sem=send_sem.at[source, m, i],
+                    recv_sem=recv_sem.at[way, item, m, i],
+                    device_id={"fs": source}, device_id_type=MESH,
+                ).wait_recv()
+
+            @pl.when(dd == k)
+            def _():
+                awaited(spot(m, l, at, source, y))
+                for other in range(1, groups):
+                    passing(source, m, i, other).start()
+
+            @pl.when(dd > k)
+            def _():
+                slot = (k - 1 - s) * (count - 1 - k) + (count - 1 - dd)
+                ref = transit.at[way, slot, m, l, pl.ds(at, piece), :]
+                awaited(ref)
+                start_hop(way, ref, relay_sem.at[way, slot, m, i], m, i, k, s, dd)
+
+    def sent(ref, sem):
+        pltpu.make_async_remote_copy(
+            src_ref=ref, dst_ref=ref, send_sem=sem, recv_sem=recv_sem.at[0, 0, 0, 0],
+            device_id={"grp": lax.rem(y + 1, groups)}, device_id_type=MESH,
+        ).wait_send()
+
+    def finish():
+        def block(t, _):
+            s, i = t // pieces, lax.rem(t, pieces)
+            l, at = cut(i)
+
+            @pl.when(s != z)
+            def _():
+                for m in range(3):
+                    for other in range(1, groups):
+                        arriving(s, m, i, other).wait_recv()
+                        passing(s, m, i, other).wait_send()
+                    sent(stage.at[s, m, l, pl.ds(at, piece), :], send_sem.at[s, m, i])
+            return 0
+
+        lax.fori_loop(0, count * pieces, block, 0)
+
+        def passed(t, _):
+            slot, i = t // pieces, lax.rem(t, pieces)
+            l, at = cut(i)
+            for way in (0, 1):
+                @pl.when(slot < z * (count - 1 - z))
+                def _():
+                    for m in range(3):
+                        sent(
+                            transit.at[way, slot, m, l, pl.ds(at, piece), :],
+                            relay_sem.at[way, slot, m, i],
+                        )
+            return 0
+
+        lax.fori_loop(0, transit.shape[1] * pieces, passed, 0)
+
+    ends = (z == 0).astype(jnp.int32) + (z == count - 1).astype(jnp.int32)
+    pl.semaphore_wait(barrier, 2 - ends + groups - 1)
+    send_phase((0, 1, 2))
+    own_block()
+    take_phase((0, 1, 2))
+    finish()
+
+
 def exchange(norm_gain, gate_weight, up_weight, down_weight, groups, count, copies, local):
     experts, rows, columns = gate_weight.shape
     width = columns // copies
@@ -222,21 +457,30 @@
     shape = (local, count * rows, width)
     dims = (groups, count, local, copies, rows, width, parts)
     pieces = local * parts
+    relaying = 1 < count <= 8 and groups > 1
+    common = [
+        pltpu.VMEM((3, local, share, width), jnp.float32),
+        pltpu.VMEM((count, 3, local, share, width), jnp.bfloat16),
+    ]
+    sem = pltpu.SemaphoreType.DMA
+    passes = [sem((count, 3, pieces, max(1, groups - 1)))] * 2
+    if relaying:
+        slots = max(1, max(k * (count - 1 - k) for k in range(count)))
+        items = max(k * (count - k) for k in range(count))
+        scratch = common + [
+            pltpu.VMEM((2, slots, 3, local, share, width), jnp.bfloat16),
+            sem((3,)), sem((count, 3, pieces)), sem((2, items, 3, pieces)),
+            sem((2, slots, 3, pieces)),
+        ] + passes
+    else:
+        scratch = common + [sem((2,))] + [sem((count, 3, pieces))] * 2 + passes
     return pl.pallas_call(
-        functools.partial(exchange_kernel, dims),
+        functools.partial(relay_kernel if relaying else exchange_kernel, dims),
         out_shape=[jax.ShapeDtypeStruct(shape, jnp.bfloat16)] * 3,
         in_specs=[pl.BlockSpec(memory_space=pltpu.VMEM)]
         + [pl.BlockSpec(memory_space=pl.ANY)] * 3,
-        out_specs=[pl.BlockSpec(memory_space=pltpu.VMEM)] * 3,
-        scratch_shapes=[
-            pltpu.VMEM((2, local, share, width), jnp.float32),
-            pltpu.VMEM((count, 3, local, share, width), jnp.bfloat16),
-            pltpu.SemaphoreType.DMA((2,)),
-            pltpu.SemaphoreType.DMA((count, 3, pieces)),
-            pltpu.SemaphoreType.DMA((count, 3, pieces)),
-            pltpu.SemaphoreType.DMA((count, 3, pieces, max(1, groups - 1))),
-            pltpu.SemaphoreType.DMA((count, 3, pieces, max(1, groups - 1))),
-        ],
+        out_specs=[pl.BlockSpec(memory_space=pl.ANY if relaying else pltpu.VMEM)] * 3,
+        scratch_shapes=scratch,
         compiler_params=pltpu.CompilerParams(
             collective_id=0, has_side_effects=True, vmem_limit_bytes=60 * 1024 * 1024
         ),

time: 480 us -> 404 us (0.84)
  Pallas kernels: 385 us -> 249 us
  starting transfers between devices: 8.64 us -> 69.6 us
    pallas_call x1, Pallas kernels: 385 us -> 249 us  [exchange(): pl.pallas_call(functools.partial(relay_kernel if relaying else exchange_k...]
    all_to_all x1, starting transfers between devices: 3.63 us -> 64.6 us  [on_device(): lax.all_to_all(summed_up.astype(jnp.bfloat16), 'fs', split_axis=0, concat...]
  transfers between devices with their start and end apart: 2 -> 2, of which waited for: 1 -> 1; matrix products, arithmetic and copies ran while one was open for 0% -> 0% of each run, Pallas kernels for 80% -> 62%
where the time goes in v2:
time: 404 us; the launch traced here: 403 us
  Pallas kernels  249 us (62%)
  starting transfers between devices  69.6 us (17%)
  blocking collectives  28.5 us (7%)
  local copies, waits for them, and re-layouts  28.1 us (7%)
  matrix products  14.9 us (4%)
  waiting for transfers between devices  9.53 us (2%)
    pallas_call x1, Pallas kernels, exchange(): pl.pallas_call(functools.partial(relay_kernel if relaying else exchange_k...  249 us
    all_to_all x1, starting transfers between devices, on_device(): lax.all_to_all(summed_up.astype(jnp.bfloat16), 'fs', split_axis=0, concat...  64.6 us
    unnamed x13, local copies, waits for them, and re-layouts  24.2 us
    all_to_all x1, blocking collectives, on_device(): lax.all_to_all(by_columns, 'tp', split_axis=3, concat_axis=3, tiled=True)  19.7 us
    all_to_all x1, waiting for transfers between devices, on_device(): lax.all_to_all(summed_up.astype(jnp.bfloat16), 'fs', split_axis=0, concat...  9.53 us
    all_gather x1, blocking collectives, on_device(): whole = lax.all_gather(tokens, 'tp', axis=1, tiled=True)  8.86 us
  transfers between devices with their start and end apart: 2, of which 1 were waited for; matrix products, arithmetic and copies ran while one was open for 0% of the time, Pallas kernels for 62%

profile of v2, /device:TPU:0, one launch (start us, length us, event | category | flops | bytes accessed | tf_op | source)
XLA Modules:
  0.0 403.5 jit_solution(2990018429495040229)
XLA Ops:
  0.6 0.8 copy.52
  1.4 0.1 eq.43
  1.6 0.1 eq.39
  1.7 0.6 reduce-window.6
  2.3 0.2 slice_reduce_fusion
  2.6 0.1 fusion.29
  2.6 0.1 reduce_sum.46
  2.8 0.1 copy.54
  2.9 0.7 compare_select_fusion
  3.6 8.9 %all_gather.3 = bf16[128,2048]{1,0:T(8,128)(2,1)S(1)} all-gather(bf16[128,512]{1,0:T(8,128)(2,1)} %param.7), channel_id=1, replica_groups=mesh['grp'=2,'fs'=4,'tp'=4] {'tp'}, dimensions={1}, use_global_device_ids=true | all-gather | bytes 655360 | tf_op jit(solution)/shard_map/all_gather | solution.py:503
  12.5 0.2 fusion.23
  12.7 1.6 convolution_convert_fusion
  14.3 0.0 copy-start
  14.3 5.0 %all-to-all-start = ((bf16[4,2,40,2048]{3,2,1,0:T(8,128)(2,1)}), bf16[4,2,40,2048]{3,2,1,0:T(8,128)(2,1)S(1)}, u32[]{:S(2)}, u32[]{:S(2)}) async-start(bf16[4,2,40,2048]{3,2,1,0:T(8,128)(2,1)} %bitcast.6), calls=%async_computation | async-start | bytes 2621440 | tf_op jit(solution)/shard_map/all_to_all | solution.py:508
  19.3 0.0 copy-done
  19.3 0.8 broadcast_in_dim.4.gains
  20.2 248.5 %shard_map.102 = (bf16[2,2048,1024]{2,1,0:T(8,128)(2,1)}, bf16[2,2048,1024]{2,1,0:T(8,128)(2,1)}, bf16[2,2048,1024]{2,1,0:T(8,128)(2,1)}) custom-call(f32[512,128]{1,0:T(8,128)} %broadcast_in_dim.4.gains, f32[8,512,1024]{2,1,0:T(8,128)} %gate_w.1, f32[8,512,1024]{2,1,0:T(8,128)} %up_w.1, f32[8,512,1024]{2,1,0:T(8,128)} %down_w.1), custom_call_target="tpu_custom_call" | custom-call | tf_op jit(solution)/shard_map/pallas_call | solution.py:477
  268.7 0.0 all-to-all-done
  268.7 0.0 slice-start
  268.7 5.0 %fusion.9 = f32[4,2,40,1024]{3,2,0,1:T(8,128)S(1)} fusion(bf16[2,2048,1024]{2,1,0:T(8,128)(2,1)} %get-tuple-element.16, bf16[4,2,40,2048]{3,2,1,0:T(8,128)(2,1)S(1)} %all-to-all-done), kind=kOutput, calls=%fused_computation.9 | convolution fusion | flops 1342177280 | bytes 11010048 | tf_op jit(solution)/shard_map/slcd,ldf->slcf/dot_general | solution.py:509
  273.8 0.0 slice-start.1
  273.8 5.3 %fusion.18 = bf16[4,2,40,1024]{3,2,0,1:T(8,128)(2,1)S(1)} fusion(bf16[2,2048,1024]{2,1,0:T(8,128)(2,1)} %get-tuple-element.17, f32[4,2,40,1024]{3,2,0,1:T(8,128)S(1)} %fusion.9, bf16[4,2,40,2048]{3,2,1,0:T(8,128)(2,1)S(1)} %all-to-all-done), kind=kOutput, calls=%fused_computation.12 | convolution fusion | flops 1344143360 | bytes 11665408 | tf_op jit(solution)/shard_map/slcd,ldf->slcf/dot_general | solution.py:510
  279.1 0.0 slice-done
  279.1 0.0 slice-done.1
  279.1 2.9 fusion.6
  282.0 0.1 copy.71
  282.2 19.7 %all_to_all.15 = bf16[4,2,40,4,512]{4,2,0,1,3:T(8,128)(2,1)S(1)} all-to-all(bf16[4,2,40,4,512]{4,2,0,1,3:T(8,128)(2,1)S(1)} %bitcast.54), channel_id=1, replica_groups=mesh['grp'=2,'fs'=4,'tp'=4] {'tp'}, dimensions={3} | all-to-all | bytes 2621440 | tf_op jit(solution)/shard_map/all_to_all | solution.py:518
  301.8 0.0 copy-start.1
  301.8 0.3 reduce_sum.48
  302.1 0.8 copy.59
  302.9 64.6 %all-to-all-start.2 = ((bf16[4,2,40,512]{3,2,1,0:T(8,128)(2,1)}), bf16[4,2,40,512]{3,2,1,0:T(8,128)(2,1)S(1)}, u32[]{:S(2)}, u32[]{:S(2)}) async-start(bf16[4,2,40,512]{3,2,1,0:T(8,128)(2,1)} %copy.59), calls=%async_computation.2 | async-start | bytes 655360 | tf_op jit(solution)/shard_map/all_to_all | solution.py:520
  367.5 0.1 copy.60
  367.6 0.1 reshape.65
  367.8 0.0 copy-done.1
  367.8 0.1 copy.51
  367.9 9.5 %all-to-all-done.2 = bf16[4,2,40,512]{3,2,1,0:T(8,128)(2,1)S(1)} async-done(((bf16[4,2,40,512]{3,2,1,0:T(8,128)(2,1)}), bf16[4,2,40,512]{3,2,1,0:T(8,128)(2,1)S(1)}, u32[]{:S(2)}, u32[]{:S(2)}) %all-to-all-start.2) | async-done | bytes 327712 | tf_op jit(solution)/shard_map/all_to_all | solution.py:520
  377.4 0.1 bitcast_convert_fusion
  377.5 1.0 gather_fusion
  378.5 0.3 reshape.64
  378.8 1.4 multiply_reduce_fusion
  380.2 7.8 %copy.75 = bf16[2,2048,1024]{2,1,0:T(8,128)(2,1)} copy(bf16[2,2048,1024]{2,1,0:T(8,128)(2,1)} %get-tuple-element.16) | data formatting | bytes 16777216
  387.9 7.8 %copy.76 = bf16[2,2048,1024]{2,1,0:T(8,128)(2,1)} copy(bf16[2,2048,1024]{2,1,0:T(8,128)(2,1)} %get-tuple-element.17) | data formatting | bytes 16777216
  395.7 7.8 %copy.77 = bf16[2,2048,1024]{2,1,0:T(8,128)(2,1)} copy(bf16[2,2048,1024]{2,1,0:T(8,128)(2,1)} %get-tuple-element.18) | data formatting | bytes 16777216
  (7 shorter events, 0.1 us)
Async XLA Ops:
  14.3 5.0 %copy-start = (f32[512]{0:T(512)S(1)}, f32[512]{0:T(512)}, u32[]{:S(2)}) copy-start(f32[512]{0:T(512)} %param.10) | copy-start | bytes 6148
  14.3 254.4 %all-to-all-start = ((bf16[4,2,40,2048]{3,2,1,0:T(8,128)(2,1)}), bf16[4,2,40,2048]{3,2,1,0:T(8,128)(2,1)S(1)}, u32[]{:S(2)}, u32[]{:S(2)}) async-start(bf16[4,2,40,2048]{3,2,1,0:T(8,128)(2,1)} %bitcast.6), calls=%async_computation | async-start | bytes 2621440 | tf_op jit(solution)/shard_map/all_to_all | solution.py:508
  268.7 10.4 %slice-start = ((s8[8388608]{0:T(1024)(128)(4,1)}), s8[4194304]{0:T(1024)(128)(4,1)S(1)}, s32[]{:S(2)}) async-start(s8[8388608]{0:T(1024)(128)(4,1)} %bitcast.52), calls=%async_computation.3 | async-start | bytes 8388608
  273.8 5.3 %slice-start.1 = ((s8[8388608]{0:T(1024)(128)(4,1)}), s8[4194304]{0:T(1024)(128)(4,1)S(1)}, s32[]{:S(2)}) async-start(s8[8388608]{0:T(1024)(128)(4,1)} %bitcast.52), calls=%async_computation.4 | async-start | bytes 8388608
  301.8 65.9 %copy-start.1 = (f32[128,2]{0,1:T(2,128)S(1)}, f32[128,2]{0,1:T(2,128)}, u32[]{:S(2)}) copy-start(f32[128,2]{0,1:T(2,128)} %param.9) | copy-start | bytes 3076
  302.9 74.5 %all-to-all-start.2 = ((bf16[4,2,40,512]{3,2,1,0:T(8,128)(2,1)}), bf16[4,2,40,512]{3,2,1,0:T(8,128)(2,1)S(1)}, u32[]{:S(2)}, u32[]{:S(2)}) async-start(bf16[4,2,40,512]{3,2,1,0:T(8,128)(2,1)} %copy.59), calls=%async_computation.2 | async-start | bytes 655360 | tf_op jit(solution)/shard_map/all_to_all | solution.py:520
